TPU v7x, 32 devices: a whole 2x2x4 slice. The times are simulated.
32 devices in a mesh: sp: 16 (over z, y, core), tp: 2 (over x).
Axes of the slice: x: 2, y: 2, z: 4, core: 2. Of those that a mesh axis runs over, the one named last changes fastest.
Arguments:
- tokens: bfloat16 [8192, 2048], P(('sp', 'tp')), may hold values from -6 to 6
- norm_gain: float32 [2048], replicated, may hold values from 0.1 to 1.9
- query_weight: bfloat16 [2048, 1024], P(None, 'tp'), may hold values from -0.13258252 to 0.13258252
- key_weight: bfloat16 [2048, 1024], P(None, 'tp'), may hold values from -0.13258252 to 0.13258252
- value_weight: bfloat16 [2048, 1024], P(None, 'tp'), may hold values from -0.125 to 0.125
- glu_value_weight: bfloat16 [2048, 1024], P(None, 'tp'), may hold values from -0.125 to 0.125
- glu_gate_weight: bfloat16 [2048, 1024], P(None, 'tp'), may hold values from -0.125 to 0.125
- qk_gain: float32 [2, 64], replicated, may hold values from 1 to 6
- mix_lambda: float32 [8], P('tp'), may hold values from 0.3 to 0.8
- head_gain: float32 [128], replicated, may hold values from 0.1 to 1.9
- conv_kernel: float32 [31, 1024], P(None, 'tp'), may hold values from -1 to 1
- channel_gain: float32 [1024], P('tp'), may hold values from 0.1 to 1.9
- channel_shift: float32 [1024], P('tp'), may hold values from -3 to 3
- output_weight: bfloat16 [2048, 2048], replicated, may hold values from -0.125 to 0.125
Outputs:
- mixed: bfloat16 [8192, 2048], P(('sp', 'tp'))
- log_totals: float32 [2, 8, 8192], P(None, 'tp', 'sp')
All inputs are finite; a program needn't handle non-finite values.
Results may differ from a plain program's by a relative error of at most 0.035.
Values may be sent and summed in bfloat16 or wider, within the bound.
A program may use at most 128 MiB of HBM per device.

v0:
```python
import math
import jax
import jax.numpy as jnp
from jax import lax
from jax.sharding import PartitionSpec as P


def from_behind(value, axis, steps):
    count = lax.axis_size(axis)
    leading, last = (max(0, -steps), min(count, count - steps))
    return lax.ppermute(value, axis, [(source, source + steps) for source in range(leading, last)])


def rotate(values, positions):
    half = values.shape[-1] // 2
    inverse = 10000.0 ** (-jnp.arange(0, half, dtype=jnp.float32) * 2.0 / values.shape[-1])
    angles = positions[:, None] * inverse[None, :]
    cosine = jnp.cos(angles)[:, None, None, :]
    sine = jnp.sin(angles)[:, None, None, :]
    first = values[..., :half]
    second = values[..., half:]
    return jnp.concatenate(
        [first * cosine - second * sine, second * cosine + first * sine], axis=-1
    )


def prepare(raw, qk_gain, positions):
    values = raw.astype(jnp.float32)
    values = values * lax.rsqrt(jnp.mean(values * values, axis=-1, keepdims=True) + 1e-06)
    values = values * qk_gain[None, None, :, :]
    return rotate(values, positions).astype(jnp.bfloat16)


def per_device(
    tokens,
    norm_gain,
    query_weight,
    key_weight,
    value_weight,
    glu_value_weight,
    glu_gate_weight,
    qk_gain,
    mix_lambda,
    head_gain,
    conv_kernel,
    channel_gain,
    channel_shift,
    output_weight,
):
    head_size = qk_gain.shape[1]
    heads_here = mix_lambda.shape[0]
    value_size = head_gain.shape[0]
    kernel_len = conv_kernel.shape[0]
    conv_here = conv_kernel.shape[1]
    width = tokens.shape[1]
    matrices = (query_weight, key_weight, value_weight, glu_value_weight, glu_gate_weight)

    def project(piece):
        inputs = piece.astype(jnp.float32)
        normed = (
            inputs
            * lax.rsqrt(jnp.mean(inputs * inputs, axis=-1, keepdims=True) + 1e-06)
            * norm_gain
        ).astype(jnp.bfloat16)
        results = [
            jnp.dot(normed, matrix, preferred_element_type=jnp.float32).astype(jnp.bfloat16)
            for matrix in matrices
        ]
        return jnp.concatenate(results, axis=1)

    projected = project(lax.all_gather(tokens, "tp", axis=0, tiled=True))
    tok_rows = projected.shape[0]
    bounds = [0]
    for matrix in matrices:
        bounds.append(bounds[-1] + matrix.shape[1])
    queries = projected[:, bounds[0] : bounds[1]].reshape(tok_rows, heads_here, 2, head_size)
    keys = projected[:, bounds[1] : bounds[2]].reshape(tok_rows, heads_here, 2, head_size)
    values = projected[:, bounds[2] : bounds[3]].reshape(tok_rows, heads_here, value_size)
    glu_a = projected[:, bounds[3] : bounds[4]]
    glu_g = projected[:, bounds[4] : bounds[5]]
    offset = lax.axis_index("sp") * tok_rows
    query_pos = offset + jnp.arange(tok_rows, dtype=jnp.int32)
    float_pos = query_pos.astype(jnp.float32)
    rq = jnp.transpose(prepare(queries, qk_gain, float_pos), (1, 2, 0, 3))
    rk = prepare(keys, qk_gain, float_pos)
    scale = head_size ** (-0.5)
    last_query = offset + tok_rows - 1
    initial = (
        jnp.full((heads_here, 2, tok_rows), -1e30, jnp.float32),
        jnp.zeros((heads_here, 2, tok_rows), jnp.float32),
        jnp.zeros((heads_here, 2, tok_rows, value_size), jnp.float32),
    )
    carry = initial
    key_piece = lax.all_gather(rk, "sp", axis=0, tiled=True)
    value_piece = lax.all_gather(values, "sp", axis=0, tiled=True)
    count = key_piece.shape[0]
    block = math.gcd(count, 512)
    blocks = count // block
    key_blocks = key_piece.reshape(blocks, block, heads_here, 2, head_size)
    value_blocks = value_piece.reshape(blocks, block, heads_here, value_size)

    def advance(state, item):
        key_block, value_block, number = item
        key_start = number * block

        def compute(inner):
            running, totals, summed = inner
            scores = (
                jnp.einsum("hmqd,khmd->hmqk", rq, key_block, preferred_element_type=jnp.float32)
                * scale
            )
            key_pos = key_start + jnp.arange(block, dtype=jnp.int32)
            allowed = key_pos[None, :] <= query_pos[:, None]
            scores = jnp.where(allowed[None, None], scores, -1e30)
            newtop = jnp.maximum(running, jnp.max(scores, axis=-1))
            probs = jnp.where(allowed[None, None], jnp.exp(scores - newtop[..., None]), 0.0)
            factor = jnp.exp(running - newtop)
            totals = totals * factor + jnp.sum(probs, axis=-1)
            added = jnp.einsum(
                "hmqk,khd->hmqd",
                probs.astype(jnp.bfloat16),
                value_block,
                preferred_element_type=jnp.float32,
            )
            return (newtop, totals, summed * factor[..., None] + added)

        def keep(inner):
            return inner

        return (lax.cond(key_start <= last_query, compute, keep, state), None)

    carry, unused = lax.scan(
        advance, carry, (key_blocks, value_blocks, jnp.arange(blocks, dtype=jnp.int32))
    )
    running, totals, summed = carry
    heads_out = (
        summed[:, 0] / totals[:, 0, :, None]
        - mix_lambda[:, None, None] * summed[:, 1] / totals[:, 1, :, None]
    )
    heads_out = (
        heads_out
        * lax.rsqrt(jnp.mean(heads_out * heads_out, axis=-1, keepdims=True) + 1e-06)
        * head_gain
    )
    attended = jnp.transpose(heads_out.astype(jnp.bfloat16), (1, 0, 2)).reshape(
        tok_rows, heads_here * value_size
    )
    log_totals = jnp.transpose(running + jnp.log(totals), (1, 0, 2))
    gated = (glu_a.astype(jnp.float32) * jax.nn.sigmoid(glu_g.astype(jnp.float32))).astype(
        jnp.bfloat16
    )
    earlier = from_behind(gated[tok_rows - (kernel_len - 1) :], "sp", 1)
    extended = jnp.concatenate([earlier, gated], axis=0).astype(jnp.float32)
    convolved = jnp.zeros((tok_rows, conv_here), jnp.float32)
    for step in range(kernel_len):
        convolved = convolved + conv_kernel[step][None, :] * extended[step : step + tok_rows]
    plain_sum, square_sum = lax.psum(
        (jnp.sum(convolved, axis=1), jnp.sum(convolved * convolved, axis=1)), "tp"
    )
    channels = conv_here * lax.axis_size("tp")
    middle = (plain_sum / channels)[:, None]
    spread = (square_sum / channels)[:, None] - middle * middle
    conv_out = jax.nn.silu(
        (convolved - middle) * lax.rsqrt(spread + 1e-05) * channel_gain + channel_shift
    ).astype(jnp.bfloat16)
    merged = jnp.concatenate([attended, conv_out], axis=1)
    groups = lax.axis_size("tp")
    branch_width = heads_here * value_size
    weight_view = output_weight.reshape(2, groups, branch_width, width)
    moved = lax.all_to_all(merged, "tp", split_axis=0, concat_axis=1, tiled=True)
    arranged = moved.reshape(tok_rows // groups, groups, 2, branch_width)
    mixed = jnp.einsum(
        "rtcj,ctjd->rd", arranged, weight_view, preferred_element_type=jnp.float32
    ).astype(jnp.bfloat16)
    return (mixed, log_totals)


def solution(mesh):
    placed = (
        P(("sp", "tp"), None),
        P(),
        P(None, "tp"),
        P(None, "tp"),
        P(None, "tp"),
        P(None, "tp"),
        P(None, "tp"),
        P(),
        P("tp"),
        P(),
        P(None, "tp"),
        P("tp"),
        P("tp"),
        P(),
    )
    return jax.shard_map(
        per_device,
        mesh=mesh,
        in_specs=placed,
        out_specs=(P(("sp", "tp"), None), P(None, "tp", "sp")),
        check_vma=False,
    )
```

profile of v0, /device:TPU:29, one launch (start us, length us, event | category | flops | bytes accessed | tf_op | source)
XLA Modules:
  0.0 434.6 jit_solution(18231954651570132200)
XLA Ops:
  8.0 35.5 %all-gather.4.cloned.1.call-done = bf16[512,2048]{1,0:T(8,128)(2,1)} async-done(((bf16[256,2048]{1,0:T(8,128)(2,1)}), bf16[512,2048]{1,0:T(8,128)(2,1)}) %all-gather.4.cloned.1.call-update) | async-done | bytes 2097168 | tf_op jit(solution)/shard_map/all_gather | solution.py:71
  43.4 2.2 fusion.20
  45.7 3.0 convolution_convert_fusion.2
  50.2 3.1 fusion.34
  56.6 3.9 fusion.31
  65.7 5.0 %fusion.77 = (f32[512]{0:T(512)S(1)}, f32[512]{0:T(512)S(1)}, f32[512,512]{1,0:T(8,128)S(1)}) fusion(f32[542,512]{1,0:T(8,128)S(1)} %maximum_convert_fusion, f32[512]{0:T(512)S(1)} %bitcast.147, f32[512]{0:T(512)S(1)} %bitcast.148, f32[512]{0:T(512)S(1)} %bitcast.150, f32[512]{0:T(512)S(1)} %bitcast.151, f32[512]{0:T(512)S(1)} %bitcast.152, ...), kind=kLoop, calls=%fused_computation.148 | loop fusion | flops 16776192 | bytes 33622016 | tf_op jit(solution)/shard_map/reduce_sum | solution.py:158
  70.7 4.4 %all-reduce = (f32[512]{0:T(512)S(1)}, f32[512]{0:T(512)S(1)}) all-reduce(f32[512]{0:T(512)S(1)} %get-tuple-element.182, f32[512]{0:T(512)S(1)} %get-tuple-element.181), channel_id=1, replica_groups=mesh['sp'=16,'tp'=2] {'tp'}, use_global_device_ids=true, to_apply=%region_13.14 | all-reduce | flops 1024 | bytes 8192 | tf_op jit(solution)/shard_map/psum | solution.py:157
  75.5 47.3 %all-gather.8.cloned.1.call-done = bf16[8192,4,128]{2,0,1:T(8,128)(2,1)} async-done(((bf16[512,4,128]{2,0,1:T(8,128)(2,1)}), bf16[8192,4,128]{2,0,1:T(8,128)(2,1)}) %all-gather.8.cloned.1.call-update) | async-done | bytes 8388624 | tf_op jit(solution)/shard_map/all_gather | solution.py:95
  122.8 7.6 %copy.23 = bf16[16,512,4,128]{3,1,2,0:T(8,128)(2,1)} copy(bf16[16,512,4,128]{3,1,0,2:T(8,128)(2,1)} %bitcast.123) | data formatting | bytes 16777216
  130.4 71.0 %all-gather.6.cloned.1.call-done = bf16[8192,4,2,64]{0,3,2,1:T(8,128)(2,1)} async-done(((bf16[512,4,2,64]{0,3,2,1:T(8,128)(2,1)}), bf16[8192,4,2,64]{0,3,2,1:T(8,128)(2,1)}) %all-gather.6.cloned.1.call-update) | async-done | bytes 8388624 | tf_op jit(solution)/shard_map/all_gather | solution.py:94
  201.4 7.9 %copy.51 = bf16[4,2,8,16,8,512]{5,4,2,1,0,3:T(8,128)(2,1)} copy(bf16[4,2,8,16,8,512]{5,4,3,2,1,0:T(8,128)(2,1)} %bitcast.124) | data formatting | bytes 16777216 | tf_op jit(solution)/shard_map/reshape | solution.py:99
  210.8 193.6 %while.15 = (s32[]{:T(128)}, f32[4,2,512]{2,1,0:T(2,128)S(1)}, f32[4,2,512]{2,1,0:T(2,128)S(1)}, f32[4,2,512,128]{3,2,1,0:T(8,128)}, s32[16]{0:T(128)S(1)}, /*in...) while((s32[]{:T(128)}, f32[4,2,512]{2,1,0:T(2,128)S(1)}, ...), condition=%wide.region_8.9_spmd.clone, body=%wide.region_3.8_spmd.clone.sunk | while | flops 833889280 | bytes 49034600 | solution.py:132
  212.1 10.8 %conditional.3 = ((f32[4,2,512]{2,1,0:T(2,128)S(1)}, f32[4,2,512]{2,1,0:T(2,128)S(1)}, f32[4,2,512,128]{3,2,1,0:T(8,128)})) conditional(s32[]{:T(128)} %convert_element_type.168, (f32[4,2,512]{2,1,0:T(2,128)S(1)}, f32[4,2,512]{2,1,0:T(2,128)S(1)}, f32[4,2,512,128]{3,2,1,0:T(8,128)}) %tuple.88, (s32[]{:T(128)}, s32[]{:T(128)}, ...), branch_computations={%region_4.4_spmd, %region_5.7_spmd} | conditional | flops 833889280 | bytes 49032288 | solution.py:130
  212.3 2.5 fusion.2
  217.0 4.6 %multiply_add_fusion = f32[4,2,512,128]{3,2,1,0:T(8,128)S(1)} fusion(f32[4,2,512,128]{3,2,1,0:T(8,128)S(1)} %copy-done.2, f32[4,2,512,512]{3,2,1,0:T(8,128)S(1)} %get-tuple-element.211, f32[4,2,512]{2,1,0:T(2,128)S(1)} %max.4, pred[512,512]{0,1:T(8,128)(4,1)S(1)} %broadcast_compare_fusion, f32[4,2,512]{2,1,0:T(2,128)S(1)} %bitcast.134, ...), kind=kOutput, calls=%fused_computation.8 | convolution fusion | flops 548405248 | bytes 13402624 | tf_op jit(solution)/shard_map/while/body/eval_jaxpr/cond/branch_1_fun/hmqk,khd->hmqd/dot_general | solution.py:119
  224.2 10.8 %conditional.3 = ((f32[4,2,512]{2,1,0:T(2,128)S(1)}, f32[4,2,512]{2,1,0:T(2,128)S(1)}, f32[4,2,512,128]{3,2,1,0:T(8,128)})) conditional(s32[]{:T(128)} %convert_element_type.168, (f32[4,2,512]{2,1,0:T(2,128)S(1)}, f32[4,2,512]{2,1,0:T(2,128)S(1)}, f32[4,2,512,128]{3,2,1,0:T(8,128)}) %tuple.88, (s32[]{:T(128)}, s32[]{:T(128)}, ...), branch_computations={%region_4.4_spmd, %region_5.7_spmd} | conditional | flops 833889280 | bytes 49032288 | solution.py:130
  224.4 2.5 fusion.2
  229.1 4.6 %multiply_add_fusion = f32[4,2,512,128]{3,2,1,0:T(8,128)S(1)} fusion(f32[4,2,512,128]{3,2,1,0:T(8,128)S(1)} %copy-done.2, f32[4,2,512,512]{3,2,1,0:T(8,128)S(1)} %get-tuple-element.211, f32[4,2,512]{2,1,0:T(2,128)S(1)} %max.4, pred[512,512]{0,1:T(8,128)(4,1)S(1)} %broadcast_compare_fusion, f32[4,2,512]{2,1,0:T(2,128)S(1)} %bitcast.134, ...), kind=kOutput, calls=%fused_computation.8 | convolution fusion | flops 548405248 | bytes 13402624 | tf_op jit(solution)/shard_map/while/body/eval_jaxpr/cond/branch_1_fun/hmqk,khd->hmqd/dot_general | solution.py:119
  236.3 10.8 %conditional.3 = ((f32[4,2,512]{2,1,0:T(2,128)S(1)}, f32[4,2,512]{2,1,0:T(2,128)S(1)}, f32[4,2,512,128]{3,2,1,0:T(8,128)})) conditional(s32[]{:T(128)} %convert_element_type.168, (f32[4,2,512]{2,1,0:T(2,128)S(1)}, f32[4,2,512]{2,1,0:T(2,128)S(1)}, f32[4,2,512,128]{3,2,1,0:T(8,128)}) %tuple.88, (s32[]{:T(128)}, s32[]{:T(128)}, ...), branch_computations={%region_4.4_spmd, %region_5.7_spmd} | conditional | flops 833889280 | bytes 49032288 | solution.py:130
  236.5 2.5 fusion.2
  241.2 4.6 %multiply_add_fusion = f32[4,2,512,128]{3,2,1,0:T(8,128)S(1)} fusion(f32[4,2,512,128]{3,2,1,0:T(8,128)S(1)} %copy-done.2, f32[4,2,512,512]{3,2,1,0:T(8,128)S(1)} %get-tuple-element.211, f32[4,2,512]{2,1,0:T(2,128)S(1)} %max.4, pred[512,512]{0,1:T(8,128)(4,1)S(1)} %broadcast_compare_fusion, f32[4,2,512]{2,1,0:T(2,128)S(1)} %bitcast.134, ...), kind=kOutput, calls=%fused_computation.8 | convolution fusion | flops 548405248 | bytes 13402624 | tf_op jit(solution)/shard_map/while/body/eval_jaxpr/cond/branch_1_fun/hmqk,khd->hmqd/dot_general | solution.py:119
  248.4 10.8 %conditional.3 = ((f32[4,2,512]{2,1,0:T(2,128)S(1)}, f32[4,2,512]{2,1,0:T(2,128)S(1)}, f32[4,2,512,128]{3,2,1,0:T(8,128)})) conditional(s32[]{:T(128)} %convert_element_type.168, (f32[4,2,512]{2,1,0:T(2,128)S(1)}, f32[4,2,512]{2,1,0:T(2,128)S(1)}, f32[4,2,512,128]{3,2,1,0:T(8,128)}) %tuple.88, (s32[]{:T(128)}, s32[]{:T(128)}, ...), branch_computations={%region_4.4_spmd, %region_5.7_spmd} | conditional | flops 833889280 | bytes 49032288 | solution.py:130
  248.6 2.5 fusion.2
  253.3 4.6 %multiply_add_fusion = f32[4,2,512,128]{3,2,1,0:T(8,128)S(1)} fusion(f32[4,2,512,128]{3,2,1,0:T(8,128)S(1)} %copy-done.2, f32[4,2,512,512]{3,2,1,0:T(8,128)S(1)} %get-tuple-element.211, f32[4,2,512]{2,1,0:T(2,128)S(1)} %max.4, pred[512,512]{0,1:T(8,128)(4,1)S(1)} %broadcast_compare_fusion, f32[4,2,512]{2,1,0:T(2,128)S(1)} %bitcast.134, ...), kind=kOutput, calls=%fused_computation.8 | convolution fusion | flops 548405248 | bytes 13402624 | tf_op jit(solution)/shard_map/while/body/eval_jaxpr/cond/branch_1_fun/hmqk,khd->hmqd/dot_general | solution.py:119
  260.5 10.8 %conditional.3 = ((f32[4,2,512]{2,1,0:T(2,128)S(1)}, f32[4,2,512]{2,1,0:T(2,128)S(1)}, f32[4,2,512,128]{3,2,1,0:T(8,128)})) conditional(s32[]{:T(128)} %convert_element_type.168, (f32[4,2,512]{2,1,0:T(2,128)S(1)}, f32[4,2,512]{2,1,0:T(2,128)S(1)}, f32[4,2,512,128]{3,2,1,0:T(8,128)}) %tuple.88, (s32[]{:T(128)}, s32[]{:T(128)}, ...), branch_computations={%region_4.4_spmd, %region_5.7_spmd} | conditional | flops 833889280 | bytes 49032288 | solution.py:130
  260.7 2.5 fusion.2
  265.4 4.6 %multiply_add_fusion = f32[4,2,512,128]{3,2,1,0:T(8,128)S(1)} fusion(f32[4,2,512,128]{3,2,1,0:T(8,128)S(1)} %copy-done.2, f32[4,2,512,512]{3,2,1,0:T(8,128)S(1)} %get-tuple-element.211, f32[4,2,512]{2,1,0:T(2,128)S(1)} %max.4, pred[512,512]{0,1:T(8,128)(4,1)S(1)} %broadcast_compare_fusion, f32[4,2,512]{2,1,0:T(2,128)S(1)} %bitcast.134, ...), kind=kOutput, calls=%fused_computation.8 | convolution fusion | flops 548405248 | bytes 13402624 | tf_op jit(solution)/shard_map/while/body/eval_jaxpr/cond/branch_1_fun/hmqk,khd->hmqd/dot_general | solution.py:119
  272.6 10.8 %conditional.3 = ((f32[4,2,512]{2,1,0:T(2,128)S(1)}, f32[4,2,512]{2,1,0:T(2,128)S(1)}, f32[4,2,512,128]{3,2,1,0:T(8,128)})) conditional(s32[]{:T(128)} %convert_element_type.168, (f32[4,2,512]{2,1,0:T(2,128)S(1)}, f32[4,2,512]{2,1,0:T(2,128)S(1)}, f32[4,2,512,128]{3,2,1,0:T(8,128)}) %tuple.88, (s32[]{:T(128)}, s32[]{:T(128)}, ...), branch_computations={%region_4.4_spmd, %region_5.7_spmd} | conditional | flops 833889280 | bytes 49032288 | solution.py:130
  272.8 2.5 fusion.2
  277.5 4.6 %multiply_add_fusion = f32[4,2,512,128]{3,2,1,0:T(8,128)S(1)} fusion(f32[4,2,512,128]{3,2,1,0:T(8,128)S(1)} %copy-done.2, f32[4,2,512,512]{3,2,1,0:T(8,128)S(1)} %get-tuple-element.211, f32[4,2,512]{2,1,0:T(2,128)S(1)} %max.4, pred[512,512]{0,1:T(8,128)(4,1)S(1)} %broadcast_compare_fusion, f32[4,2,512]{2,1,0:T(2,128)S(1)} %bitcast.134, ...), kind=kOutput, calls=%fused_computation.8 | convolution fusion | flops 548405248 | bytes 13402624 | tf_op jit(solution)/shard_map/while/body/eval_jaxpr/cond/branch_1_fun/hmqk,khd->hmqd/dot_general | solution.py:119
  284.7 10.8 %conditional.3 = ((f32[4,2,512]{2,1,0:T(2,128)S(1)}, f32[4,2,512]{2,1,0:T(2,128)S(1)}, f32[4,2,512,128]{3,2,1,0:T(8,128)})) conditional(s32[]{:T(128)} %convert_element_type.168, (f32[4,2,512]{2,1,0:T(2,128)S(1)}, f32[4,2,512]{2,1,0:T(2,128)S(1)}, f32[4,2,512,128]{3,2,1,0:T(8,128)}) %tuple.88, (s32[]{:T(128)}, s32[]{:T(128)}, ...), branch_computations={%region_4.4_spmd, %region_5.7_spmd} | conditional | flops 833889280 | bytes 49032288 | solution.py:130
  284.9 2.5 fusion.2
  289.6 4.6 %multiply_add_fusion = f32[4,2,512,128]{3,2,1,0:T(8,128)S(1)} fusion(f32[4,2,512,128]{3,2,1,0:T(8,128)S(1)} %copy-done.2, f32[4,2,512,512]{3,2,1,0:T(8,128)S(1)} %get-tuple-element.211, f32[4,2,512]{2,1,0:T(2,128)S(1)} %max.4, pred[512,512]{0,1:T(8,128)(4,1)S(1)} %broadcast_compare_fusion, f32[4,2,512]{2,1,0:T(2,128)S(1)} %bitcast.134, ...), kind=kOutput, calls=%fused_computation.8 | convolution fusion | flops 548405248 | bytes 13402624 | tf_op jit(solution)/shard_map/while/body/eval_jaxpr/cond/branch_1_fun/hmqk,khd->hmqd/dot_general | solution.py:119
  296.8 10.8 %conditional.3 = ((f32[4,2,512]{2,1,0:T(2,128)S(1)}, f32[4,2,512]{2,1,0:T(2,128)S(1)}, f32[4,2,512,128]{3,2,1,0:T(8,128)})) conditional(s32[]{:T(128)} %convert_element_type.168, (f32[4,2,512]{2,1,0:T(2,128)S(1)}, f32[4,2,512]{2,1,0:T(2,128)S(1)}, f32[4,2,512,128]{3,2,1,0:T(8,128)}) %tuple.88, (s32[]{:T(128)}, s32[]{:T(128)}, ...), branch_computations={%region_4.4_spmd, %region_5.7_spmd} | conditional | flops 833889280 | bytes 49032288 | solution.py:130
  297.0 2.5 fusion.2
  301.7 4.6 %multiply_add_fusion = f32[4,2,512,128]{3,2,1,0:T(8,128)S(1)} fusion(f32[4,2,512,128]{3,2,1,0:T(8,128)S(1)} %copy-done.2, f32[4,2,512,512]{3,2,1,0:T(8,128)S(1)} %get-tuple-element.211, f32[4,2,512]{2,1,0:T(2,128)S(1)} %max.4, pred[512,512]{0,1:T(8,128)(4,1)S(1)} %broadcast_compare_fusion, f32[4,2,512]{2,1,0:T(2,128)S(1)} %bitcast.134, ...), kind=kOutput, calls=%fused_computation.8 | convolution fusion | flops 548405248 | bytes 13402624 | tf_op jit(solution)/shard_map/while/body/eval_jaxpr/cond/branch_1_fun/hmqk,khd->hmqd/dot_general | solution.py:119
  308.9 10.8 %conditional.3 = ((f32[4,2,512]{2,1,0:T(2,128)S(1)}, f32[4,2,512]{2,1,0:T(2,128)S(1)}, f32[4,2,512,128]{3,2,1,0:T(8,128)})) conditional(s32[]{:T(128)} %convert_element_type.168, (f32[4,2,512]{2,1,0:T(2,128)S(1)}, f32[4,2,512]{2,1,0:T(2,128)S(1)}, f32[4,2,512,128]{3,2,1,0:T(8,128)}) %tuple.88, (s32[]{:T(128)}, s32[]{:T(128)}, ...), branch_computations={%region_4.4_spmd, %region_5.7_spmd} | conditional | flops 833889280 | bytes 49032288 | solution.py:130
  309.1 2.5 fusion.2
  313.8 4.6 %multiply_add_fusion = f32[4,2,512,128]{3,2,1,0:T(8,128)S(1)} fusion(f32[4,2,512,128]{3,2,1,0:T(8,128)S(1)} %copy-done.2, f32[4,2,512,512]{3,2,1,0:T(8,128)S(1)} %get-tuple-element.211, f32[4,2,512]{2,1,0:T(2,128)S(1)} %max.4, pred[512,512]{0,1:T(8,128)(4,1)S(1)} %broadcast_compare_fusion, f32[4,2,512]{2,1,0:T(2,128)S(1)} %bitcast.134, ...), kind=kOutput, calls=%fused_computation.8 | convolution fusion | flops 548405248 | bytes 13402624 | tf_op jit(solution)/shard_map/while/body/eval_jaxpr/cond/branch_1_fun/hmqk,khd->hmqd/dot_general | solution.py:119
  321.0 10.8 %conditional.3 = ((f32[4,2,512]{2,1,0:T(2,128)S(1)}, f32[4,2,512]{2,1,0:T(2,128)S(1)}, f32[4,2,512,128]{3,2,1,0:T(8,128)})) conditional(s32[]{:T(128)} %convert_element_type.168, (f32[4,2,512]{2,1,0:T(2,128)S(1)}, f32[4,2,512]{2,1,0:T(2,128)S(1)}, f32[4,2,512,128]{3,2,1,0:T(8,128)}) %tuple.88, (s32[]{:T(128)}, s32[]{:T(128)}, ...), branch_computations={%region_4.4_spmd, %region_5.7_spmd} | conditional | flops 833889280 | bytes 49032288 | solution.py:130
  321.2 2.5 fusion.2
  325.9 4.6 %multiply_add_fusion = f32[4,2,512,128]{3,2,1,0:T(8,128)S(1)} fusion(f32[4,2,512,128]{3,2,1,0:T(8,128)S(1)} %copy-done.2, f32[4,2,512,512]{3,2,1,0:T(8,128)S(1)} %get-tuple-element.211, f32[4,2,512]{2,1,0:T(2,128)S(1)} %max.4, pred[512,512]{0,1:T(8,128)(4,1)S(1)} %broadcast_compare_fusion, f32[4,2,512]{2,1,0:T(2,128)S(1)} %bitcast.134, ...), kind=kOutput, calls=%fused_computation.8 | convolution fusion | flops 548405248 | bytes 13402624 | tf_op jit(solution)/shard_map/while/body/eval_jaxpr/cond/branch_1_fun/hmqk,khd->hmqd/dot_general | solution.py:119
  333.1 10.8 %conditional.3 = ((f32[4,2,512]{2,1,0:T(2,128)S(1)}, f32[4,2,512]{2,1,0:T(2,128)S(1)}, f32[4,2,512,128]{3,2,1,0:T(8,128)})) conditional(s32[]{:T(128)} %convert_element_type.168, (f32[4,2,512]{2,1,0:T(2,128)S(1)}, f32[4,2,512]{2,1,0:T(2,128)S(1)}, f32[4,2,512,128]{3,2,1,0:T(8,128)}) %tuple.88, (s32[]{:T(128)}, s32[]{:T(128)}, ...), branch_computations={%region_4.4_spmd, %region_5.7_spmd} | conditional | flops 833889280 | bytes 49032288 | solution.py:130
  333.3 2.5 fusion.2
  338.0 4.6 %multiply_add_fusion = f32[4,2,512,128]{3,2,1,0:T(8,128)S(1)} fusion(f32[4,2,512,128]{3,2,1,0:T(8,128)S(1)} %copy-done.2, f32[4,2,512,512]{3,2,1,0:T(8,128)S(1)} %get-tuple-element.211, f32[4,2,512]{2,1,0:T(2,128)S(1)} %max.4, pred[512,512]{0,1:T(8,128)(4,1)S(1)} %broadcast_compare_fusion, f32[4,2,512]{2,1,0:T(2,128)S(1)} %bitcast.134, ...), kind=kOutput, calls=%fused_computation.8 | convolution fusion | flops 548405248 | bytes 13402624 | tf_op jit(solution)/shard_map/while/body/eval_jaxpr/cond/branch_1_fun/hmqk,khd->hmqd/dot_general | solution.py:119
  345.2 10.8 %conditional.3 = ((f32[4,2,512]{2,1,0:T(2,128)S(1)}, f32[4,2,512]{2,1,0:T(2,128)S(1)}, f32[4,2,512,128]{3,2,1,0:T(8,128)})) conditional(s32[]{:T(128)} %convert_element_type.168, (f32[4,2,512]{2,1,0:T(2,128)S(1)}, f32[4,2,512]{2,1,0:T(2,128)S(1)}, f32[4,2,512,128]{3,2,1,0:T(8,128)}) %tuple.88, (s32[]{:T(128)}, s32[]{:T(128)}, ...), branch_computations={%region_4.4_spmd, %region_5.7_spmd} | conditional | flops 833889280 | bytes 49032288 | solution.py:130
  345.4 2.5 fusion.2
  350.1 4.6 %multiply_add_fusion = f32[4,2,512,128]{3,2,1,0:T(8,128)S(1)} fusion(f32[4,2,512,128]{3,2,1,0:T(8,128)S(1)} %copy-done.2, f32[4,2,512,512]{3,2,1,0:T(8,128)S(1)} %get-tuple-element.211, f32[4,2,512]{2,1,0:T(2,128)S(1)} %max.4, pred[512,512]{0,1:T(8,128)(4,1)S(1)} %broadcast_compare_fusion, f32[4,2,512]{2,1,0:T(2,128)S(1)} %bitcast.134, ...), kind=kOutput, calls=%fused_computation.8 | convolution fusion | flops 548405248 | bytes 13402624 | tf_op jit(solution)/shard_map/while/body/eval_jaxpr/cond/branch_1_fun/hmqk,khd->hmqd/dot_general | solution.py:119
  357.3 10.8 %conditional.3 = ((f32[4,2,512]{2,1,0:T(2,128)S(1)}, f32[4,2,512]{2,1,0:T(2,128)S(1)}, f32[4,2,512,128]{3,2,1,0:T(8,128)})) conditional(s32[]{:T(128)} %convert_element_type.168, (f32[4,2,512]{2,1,0:T(2,128)S(1)}, f32[4,2,512]{2,1,0:T(2,128)S(1)}, f32[4,2,512,128]{3,2,1,0:T(8,128)}) %tuple.88, (s32[]{:T(128)}, s32[]{:T(128)}, ...), branch_computations={%region_4.4_spmd, %region_5.7_spmd} | conditional | flops 833889280 | bytes 49032288 | solution.py:130
  357.5 2.5 fusion.2
  362.2 4.6 %multiply_add_fusion = f32[4,2,512,128]{3,2,1,0:T(8,128)S(1)} fusion(f32[4,2,512,128]{3,2,1,0:T(8,128)S(1)} %copy-done.2, f32[4,2,512,512]{3,2,1,0:T(8,128)S(1)} %get-tuple-element.211, f32[4,2,512]{2,1,0:T(2,128)S(1)} %max.4, pred[512,512]{0,1:T(8,128)(4,1)S(1)} %broadcast_compare_fusion, f32[4,2,512]{2,1,0:T(2,128)S(1)} %bitcast.134, ...), kind=kOutput, calls=%fused_computation.8 | convolution fusion | flops 548405248 | bytes 13402624 | tf_op jit(solution)/shard_map/while/body/eval_jaxpr/cond/branch_1_fun/hmqk,khd->hmqd/dot_general | solution.py:119
  369.4 10.8 %conditional.3 = ((f32[4,2,512]{2,1,0:T(2,128)S(1)}, f32[4,2,512]{2,1,0:T(2,128)S(1)}, f32[4,2,512,128]{3,2,1,0:T(8,128)})) conditional(s32[]{:T(128)} %convert_element_type.168, (f32[4,2,512]{2,1,0:T(2,128)S(1)}, f32[4,2,512]{2,1,0:T(2,128)S(1)}, f32[4,2,512,128]{3,2,1,0:T(8,128)}) %tuple.88, (s32[]{:T(128)}, s32[]{:T(128)}, ...), branch_computations={%region_4.4_spmd, %region_5.7_spmd} | conditional | flops 833889280 | bytes 49032288 | solution.py:130
  369.6 2.5 fusion.2
  374.3 4.6 %multiply_add_fusion = f32[4,2,512,128]{3,2,1,0:T(8,128)S(1)} fusion(f32[4,2,512,128]{3,2,1,0:T(8,128)S(1)} %copy-done.2, f32[4,2,512,512]{3,2,1,0:T(8,128)S(1)} %get-tuple-element.211, f32[4,2,512]{2,1,0:T(2,128)S(1)} %max.4, pred[512,512]{0,1:T(8,128)(4,1)S(1)} %broadcast_compare_fusion, f32[4,2,512]{2,1,0:T(2,128)S(1)} %bitcast.134, ...), kind=kOutput, calls=%fused_computation.8 | convolution fusion | flops 548405248 | bytes 13402624 | tf_op jit(solution)/shard_map/while/body/eval_jaxpr/cond/branch_1_fun/hmqk,khd->hmqd/dot_general | solution.py:119
  381.5 10.8 %conditional.3 = ((f32[4,2,512]{2,1,0:T(2,128)S(1)}, f32[4,2,512]{2,1,0:T(2,128)S(1)}, f32[4,2,512,128]{3,2,1,0:T(8,128)})) conditional(s32[]{:T(128)} %convert_element_type.168, (f32[4,2,512]{2,1,0:T(2,128)S(1)}, f32[4,2,512]{2,1,0:T(2,128)S(1)}, f32[4,2,512,128]{3,2,1,0:T(8,128)}) %tuple.88, (s32[]{:T(128)}, s32[]{:T(128)}, ...), branch_computations={%region_4.4_spmd, %region_5.7_spmd} | conditional | flops 833889280 | bytes 49032288 | solution.py:130
  381.7 2.5 fusion.2
  386.4 4.6 %multiply_add_fusion = f32[4,2,512,128]{3,2,1,0:T(8,128)S(1)} fusion(f32[4,2,512,128]{3,2,1,0:T(8,128)S(1)} %copy-done.2, f32[4,2,512,512]{3,2,1,0:T(8,128)S(1)} %get-tuple-element.211, f32[4,2,512]{2,1,0:T(2,128)S(1)} %max.4, pred[512,512]{0,1:T(8,128)(4,1)S(1)} %broadcast_compare_fusion, f32[4,2,512]{2,1,0:T(2,128)S(1)} %bitcast.134, ...), kind=kOutput, calls=%fused_computation.8 | convolution fusion | flops 548405248 | bytes 13402624 | tf_op jit(solution)/shard_map/while/body/eval_jaxpr/cond/branch_1_fun/hmqk,khd->hmqd/dot_general | solution.py:119
  393.6 10.8 %conditional.3 = ((f32[4,2,512]{2,1,0:T(2,128)S(1)}, f32[4,2,512]{2,1,0:T(2,128)S(1)}, f32[4,2,512,128]{3,2,1,0:T(8,128)})) conditional(s32[]{:T(128)} %convert_element_type.168, (f32[4,2,512]{2,1,0:T(2,128)S(1)}, f32[4,2,512]{2,1,0:T(2,128)S(1)}, f32[4,2,512,128]{3,2,1,0:T(8,128)}) %tuple.88, (s32[]{:T(128)}, s32[]{:T(128)}, ...), branch_computations={%region_4.4_spmd, %region_5.7_spmd} | conditional | flops 833889280 | bytes 49032288 | solution.py:130
  393.8 2.5 fusion.2
  398.5 4.6 %multiply_add_fusion = f32[4,2,512,128]{3,2,1,0:T(8,128)S(1)} fusion(f32[4,2,512,128]{3,2,1,0:T(8,128)S(1)} %copy-done.2, f32[4,2,512,512]{3,2,1,0:T(8,128)S(1)} %get-tuple-element.211, f32[4,2,512]{2,1,0:T(2,128)S(1)} %max.4, pred[512,512]{0,1:T(8,128)(4,1)S(1)} %broadcast_compare_fusion, f32[4,2,512]{2,1,0:T(2,128)S(1)} %bitcast.134, ...), kind=kOutput, calls=%fused_computation.8 | convolution fusion | flops 548405248 | bytes 13402624 | tf_op jit(solution)/shard_map/while/body/eval_jaxpr/cond/branch_1_fun/hmqk,khd->hmqd/dot_general | solution.py:119
  404.5 2.3 multiply_reduce_fusion.1
  408.9 3.6 all-to-all-start
  413.1 7.6 %all-to-all-done = bf16[2,256,1024]{2,1,0:T(8,128)(2,1)S(1)} async-done(((bf16[2,256,1024]{2,1,0:T(8,128)(2,1)}), bf16[2,256,1024]{2,1,0:T(8,128)(2,1)S(1)}, u32[]{:S(2)}, u32[]{:S(2)}) %all-to-all-start) | async-done | bytes 1048608 | tf_op jit(solution)/shard_map/all_to_all | solution.py:170
  421.2 6.8 %fusion.23 = bf16[256,2048]{1,0:T(8,128)(2,1)} fusion(bf16[2,2,512,2048]{3,2,1,0:T(8,128)(2,1)} %bitcast.122, bf16[256,2,2,512]{0,3,2,1:T(8,128)(2,1)S(1)} %bitcast.126), kind=kOutput, calls=%fused_computation.31 | convolution fusion | flops 2148007936 | bytes 10485760 | tf_op jit(solution)/shard_map/rtcj,ctjd->rd/dot_general | solution.py:172
  (260 shorter events, 83.6 us)
Async XLA Ops:
  7.2 43.0 %copy-start = (bf16[2048,512]{1,0:T(8,128)(2,1)S(1)}, bf16[2048,512]{1,0:T(8,128)(2,1)}, u32[]{:S(2)}) copy-start(bf16[2048,512]{1,0:T(8,128)(2,1)} %param.20) | copy-start | bytes 6291460
  7.2 38.5 %copy-start.15 = (f32[2048]{0:T(1024)S(1)}, f32[2048]{0:T(1024)}, u32[]{:S(2)}) copy-start(f32[2048]{0:T(1024)} %param.19) | copy-start | bytes 24580
  7.2 36.2 %all-gather.4.cloned.1.call-start = ((), (), s32[]{:S(2)}) async-start(), calls=%async_computation.1 | async-start | bytes 3145728 | tf_op jit(solution)/shard_map/all_gather | solution.py:71
  7.9 114.9 %all-gather.8.cloned.1.call-start = ((), (), s32[]{:S(2)}) async-start(), calls=%async_computation.3 | async-start | bytes 8912896 | tf_op jit(solution)/shard_map/all_gather | solution.py:95
  43.4 2.2 copy-start.4
  49.7 151.6 %all-gather.6.cloned.1.call-start = ((), (), s32[]{:S(2)}) async-start(), calls=%async_computation.2 | async-start | bytes 8912896 | tf_op jit(solution)/shard_map/all_gather | solution.py:94
  50.1 3.2 copy-start.5
  50.2 3.2 copy-start.13
  53.3 1.5 copy-start.10
  55.2 1.2 copy-start.7
  56.5 4.0 copy-start.6
  56.5 4.0 copy-start.14
  62.0 3.4 collective-permute-start
  65.6 9.4 %copy-start.8 = (f32[512]{0:T(512)S(1)}, f32[512]{0:T(512)}, u32[]{:S(2)}) copy-start(f32[512]{0:T(512)} %param.30) | copy-start | bytes 6148
  65.7 9.4 %copy-start.9 = (f32[512]{0:T(512)S(1)}, f32[512]{0:T(512)}, u32[]{:S(2)}) copy-start(f32[512]{0:T(512)} %param.29) | copy-start | bytes 6148
  210.8 193.7 %copy-start.12 = (f32[4]{0:T(128)S(1)}, f32[4]{0:T(128)}, u32[]{:S(2)}) copy-start(f32[4]{0:T(128)} %param.26) | copy-start | bytes 52
  214.9 2.1 copy-start.2
  221.6 1.3 copy-start.3
  227.0 2.1 copy-start.2
  233.7 1.3 copy-start.3
  239.1 2.1 copy-start.2
  245.8 1.3 copy-start.3
  251.2 2.1 copy-start.2
  257.9 1.3 copy-start.3
  263.3 2.1 copy-start.2
  270.0 1.3 copy-start.3
  275.4 2.1 copy-start.2
  282.1 1.3 copy-start.3
  287.5 2.1 copy-start.2
  294.2 1.3 copy-start.3
  299.6 2.1 copy-start.2
  306.3 1.3 copy-start.3
  311.7 2.1 copy-start.2
  318.4 1.3 copy-start.3
  323.8 2.1 copy-start.2
  330.5 1.3 copy-start.3
  335.9 2.1 copy-start.2
  342.6 1.3 copy-start.3
  348.0 2.1 copy-start.2
  354.7 1.3 copy-start.3
  360.1 2.1 copy-start.2
  366.8 1.3 copy-start.3
  372.2 2.1 copy-start.2
  378.9 1.3 copy-start.3
  384.3 2.1 copy-start.2
  391.0 1.3 copy-start.3
  396.4 2.1 copy-start.2
  403.1 1.3 copy-start.3
  404.4 2.3 copy-start.11
  408.9 11.8 %all-to-all-start = ((bf16[2,256,1024]{2,1,0:T(8,128)(2,1)}), bf16[2,256,1024]{2,1,0:T(8,128)(2,1)S(1)}, u32[]{:S(2)}, u32[]{:S(2)}) async-start(bf16[2,256,1024]{2,1,0:T(8,128)(2,1)} %pad_maximum_fusion), calls=%async_computation | async-start | bytes 2097152 | tf_op jit(solution)/shard_map/all_to_all | solution.py:170
  421.2 6.9 %copy-start.1 = (bf16[2048,512]{1,0:T(8,128)(2,1)S(1)}, bf16[2048,512]{1,0:T(8,128)(2,1)}, u32[]{:S(2)}) copy-start(bf16[2048,512]{1,0:T(8,128)(2,1)} %param.20) | copy-start | bytes 6291460
Sparse Core Ops, SparseCore 0:
  9.5 33.8 all-gather.3
  49.9 72.8 all-gather.7
  125.5 75.8 all-gather.5
where the time goes:
time: 437 us; the launch traced here: 435 us
  waiting for transfers between devices  164 us (38%)
  matrix products  134 us (31%)
  other arithmetic  50.9 us (12%)
  local copies, waits for them, and re-layouts  50.6 us (12%)
  between operations  14.1 us (3%)
  loops' own time  11.9 us (3%)
  starting transfers between devices  4.99 us (1%)
    dot_general x16, matrix products, compute(): jnp.einsum('hmqk,khd->hmqd', probs.astype(jnp.bfloat16), value_block, pre...  73.1 us
    all_gather x1, waiting for transfers between devices, per_device(): key_piece = lax.all_gather(rk, 'sp', axis=0, tiled=True)  71 us
    all_gather x1, waiting for transfers between devices, per_device(): value_piece = lax.all_gather(values, 'sp', axis=0, tiled=True)  47.3 us
    dot_general x16, matrix products, compute(): jnp.einsum('hmqd,khmd->hmqk', rq, key_block, preferred_element_type=jnp.f...  40.7 us
    all_gather x1, waiting for transfers between devices, per_device(): projected = project(lax.all_gather(tokens, 'tp', axis=0, tiled=True))  35.5 us
    reduce_sum x16, other arithmetic, compute(): totals = totals * factor + jnp.sum(probs, axis=-1)  32.8 us
    cond x80, local copies, waits for them, and re-layouts  21.3 us
    dot_general x5, matrix products, project(): jnp.dot(normed, matrix, preferred_element_type=jnp.float32)  13.1 us
  transfers between devices with their start and end apart: 5, of which 5 were waited for; matrix products, arithmetic and copies ran while one was open for 6% of the time, Pallas kernels for 0%

commit v1 on v0

--- a/solution.py
+++ b/solution.py
@@ -3,6 +3,16 @@
 import jax.numpy as jnp
 from jax import lax
 from jax.sharding import PartitionSpec as P
+
+
+def turned_line(array, name, dim):
+    size = lax.axis_size(name)
+    current, tiles = (array, [array])
+    for _ in range(size - 1):
+        current = lax.ppermute(current, name, [(i, (i + 1) % size) for i in range(size)])
+        tiles.insert(0, current)
+    flat = jnp.concatenate(tiles, axis=dim)
+    return jnp.roll(flat, (lax.axis_index(name) + 1) * array.shape[dim], axis=dim)
 
 
 def from_behind(value, axis, steps):
@@ -92,7 +102,7 @@
     )
     carry = initial
     key_piece = lax.all_gather(rk, "sp", axis=0, tiled=True)
-    value_piece = lax.all_gather(values, "sp", axis=0, tiled=True)
+    value_piece = turned_line(values, "sp", 0)
     count = key_piece.shape[0]
     block = math.gcd(count, 512)
     blocks = count // block

time: 437 us -> 566 us (1.30)
  starting transfers between devices: 4.99 us -> 78.5 us
  local copies, waits for them, and re-layouts: 50.6 us -> 107 us
  waiting for transfers between devices: 164 us -> 155 us
    ppermute x0 -> x15, waiting for transfers between devices: none -> 110 us  [turned_line(): lax.ppermute(current, name, [(i, (i + 1) % size) for i in range(size)])]
    ppermute x0 -> x15, starting transfers between devices: none -> 73.6 us  [turned_line(): lax.ppermute(current, name, [(i, (i + 1) % size) for i in range(size)])]
    all_gather x1, waiting for transfers between devices: 71 us -> 0.01 us  [per_device(): key_piece = lax.all_gather(rk, 'sp', axis=0, tiled=True)]
    unnamed x31 -> x128, local copies, waits for them, and re-layouts: 7.74 us -> 55.6 us
    all_gather x1 -> x0, waiting for transfers between devices: 47.3 us -> none  [per_device(): value_piece = lax.all_gather(values, 'sp', axis=0, tiled=True)]
    dynamic_slice x0 -> x1, local copies, waits for them, and re-layouts: none -> 7.18 us  [turned_line(): jnp.roll(flat, (lax.axis_index(name) + 1) * array.shape[dim], axis=dim)]
  transfers between devices with their start and end apart: 5 -> 19, of which waited for: 5 -> 17; matrix products, arithmetic and copies ran while one was open for 6% -> 13% of each run, Pallas kernels for 0% -> 0%
where the time goes in v1:
time: 566 us; the launch traced here: 564 us
  waiting for transfers between devices  155 us (27%)
  matrix products  138 us (24%)
  local copies, waits for them, and re-layouts  107 us (19%)
  starting transfers between devices  78.5 us (14%)
  other arithmetic  54.5 us (10%)
  between operations  14.7 us (3%)
  loops' own time  12.4 us (2%)
    ppermute x15, waiting for transfers between devices, turned_line(): lax.ppermute(current, name, [(i, (i + 1) % size) for i in range(size)])  110 us
    ppermute x15, starting transfers between devices, turned_line(): lax.ppermute(current, name, [(i, (i + 1) % size) for i in range(size)])  73.6 us
    dot_general x16, matrix products, compute(): jnp.einsum('hmqk,khd->hmqd', probs.astype(jnp.bfloat16), value_block, pre...  73.1 us
    unnamed x128, local copies, waits for them, and re-layouts  55.6 us
    dot_general x16, matrix products, compute(): jnp.einsum('hmqd,khmd->hmqk', rq, key_block, preferred_element_type=jnp.f...  43 us
    all_gather x1, waiting for transfers between devices, per_device(): projected = project(lax.all_gather(tokens, 'tp', axis=0, tiled=True))  35.1 us
    reduce_sum x16, other arithmetic, compute(): totals = totals * factor + jnp.sum(probs, axis=-1)  32.8 us
    cond x80, local copies, waits for them, and re-layouts  21.4 us
  transfers between devices with their start and end apart: 19, of which 17 were waited for; matrix products, arithmetic and copies ran while one was open for 13% of the time, Pallas kernels for 0%

profile of v1, /device:TPU:29, one launch (start us, length us, event | category | flops | bytes accessed | tf_op | source)
XLA Modules:
  0.0 563.9 jit_solution(9157541417747441586)
XLA Ops:
  8.3 35.1 %all-gather.3.cloned.1.call-done = bf16[512,2048]{1,0:T(8,128)(2,1)} async-done(((bf16[256,2048]{1,0:T(8,128)(2,1)}), bf16[512,2048]{1,0:T(8,128)(2,1)}) %all-gather.3.cloned.1.call-update) | async-done | bytes 2097168 | tf_op jit(solution)/shard_map/all_gather | solution.py:81
  57.6 9.0 %collective-permute-done = bf16[512,4,128]{2,0,1:T(8,128)(2,1)S(1)} collective-permute-done((bf16[512,4,128]{2,0,1:T(8,128)(2,1)S(1)}, bf16[512,4,128]{2,0,1:T(8,128)(2,1)S(1)}, u32[]{:S(2)}, u32[]{:S(2)}) %collective-permute-start) | collective-permute-done | bytes 524320 | tf_op jit(solution)/shard_map/ppermute | solution.py:12
  66.6 5.2 collective-permute-start.1
  71.8 16.9 %collective-permute-done.1 = bf16[512,4,128]{2,0,1:T(8,128)(2,1)S(1)} collective-permute-done((bf16[512,4,128]{2,0,1:T(8,128)(2,1)S(1)}, bf16[512,4,128]{2,0,1:T(8,128)(2,1)S(1)}, u32[]{:S(2)}, u32[]{:S(2)}) %collective-permute-start.1) | collective-permute-done | bytes 524320 | tf_op jit(solution)/shard_map/ppermute | solution.py:12
  89.5 5.2 collective-permute-start.2
  94.7 16.6 %collective-permute-done.2 = bf16[512,4,128]{2,0,1:T(8,128)(2,1)S(1)} collective-permute-done((bf16[512,4,128]{2,0,1:T(8,128)(2,1)S(1)}, bf16[512,4,128]{2,0,1:T(8,128)(2,1)S(1)}, u32[]{:S(2)}, u32[]{:S(2)}) %collective-permute-start.2) | collective-permute-done | bytes 524320 | tf_op jit(solution)/shard_map/ppermute | solution.py:12
  112.0 5.2 collective-permute-start.3
  117.2 15.8 %collective-permute-done.3 = bf16[512,4,128]{2,0,1:T(8,128)(2,1)S(1)} collective-permute-done((bf16[512,4,128]{2,0,1:T(8,128)(2,1)S(1)}, bf16[512,4,128]{2,0,1:T(8,128)(2,1)S(1)}, u32[]{:S(2)}, u32[]{:S(2)}) %collective-permute-start.3) | collective-permute-done | bytes 524320 | tf_op jit(solution)/shard_map/ppermute | solution.py:12
  133.8 5.2 collective-permute-start.4
  139.0 6.9 %collective-permute-done.4 = bf16[512,4,128]{2,0,1:T(8,128)(2,1)S(1)} collective-permute-done((bf16[512,4,128]{2,0,1:T(8,128)(2,1)S(1)}, bf16[512,4,128]{2,0,1:T(8,128)(2,1)S(1)}, u32[]{:S(2)}, u32[]{:S(2)}) %collective-permute-start.4) | collective-permute-done | bytes 524320 | tf_op jit(solution)/shard_map/ppermute | solution.py:12
  146.6 5.2 collective-permute-start.5
  151.8 6.1 %collective-permute-done.5 = bf16[512,4,128]{2,0,1:T(8,128)(2,1)S(1)} collective-permute-done((bf16[512,4,128]{2,0,1:T(8,128)(2,1)S(1)}, bf16[512,4,128]{2,0,1:T(8,128)(2,1)S(1)}, u32[]{:S(2)}, u32[]{:S(2)}) %collective-permute-start.5) | collective-permute-done | bytes 524320 | tf_op jit(solution)/shard_map/ppermute | solution.py:12
  158.8 5.2 collective-permute-start.6
  163.9 6.1 %collective-permute-done.6 = bf16[512,4,128]{2,0,1:T(8,128)(2,1)S(1)} collective-permute-done((bf16[512,4,128]{2,0,1:T(8,128)(2,1)S(1)}, bf16[512,4,128]{2,0,1:T(8,128)(2,1)S(1)}, u32[]{:S(2)}, u32[]{:S(2)}) %collective-permute-start.6) | collective-permute-done | bytes 524320 | tf_op jit(solution)/shard_map/ppermute | solution.py:12
  170.9 5.2 collective-permute-start.7
  176.0 6.1 %collective-permute-done.7 = bf16[512,4,128]{2,0,1:T(8,128)(2,1)S(1)} collective-permute-done((bf16[512,4,128]{2,0,1:T(8,128)(2,1)S(1)}, bf16[512,4,128]{2,0,1:T(8,128)(2,1)S(1)}, u32[]{:S(2)}, u32[]{:S(2)}) %collective-permute-start.7) | collective-permute-done | bytes 524320 | tf_op jit(solution)/shard_map/ppermute | solution.py:12
  183.0 5.2 collective-permute-start.8
  188.1 6.1 %collective-permute-done.8 = bf16[512,4,128]{2,0,1:T(8,128)(2,1)S(1)} collective-permute-done((bf16[512,4,128]{2,0,1:T(8,128)(2,1)S(1)}, bf16[512,4,128]{2,0,1:T(8,128)(2,1)S(1)}, u32[]{:S(2)}, u32[]{:S(2)}) %collective-permute-start.8) | collective-permute-done | bytes 524320 | tf_op jit(solution)/shard_map/ppermute | solution.py:12
  195.0 5.2 collective-permute-start.9
  200.2 6.1 %collective-permute-done.9 = bf16[512,4,128]{2,0,1:T(8,128)(2,1)S(1)} collective-permute-done((bf16[512,4,128]{2,0,1:T(8,128)(2,1)S(1)}, bf16[512,4,128]{2,0,1:T(8,128)(2,1)S(1)}, u32[]{:S(2)}, u32[]{:S(2)}) %collective-permute-start.9) | collective-permute-done | bytes 524320 | tf_op jit(solution)/shard_map/ppermute | solution.py:12
  207.1 5.2 collective-permute-start.10
  212.3 6.1 %collective-permute-done.10 = bf16[512,4,128]{2,0,1:T(8,128)(2,1)S(1)} collective-permute-done((bf16[512,4,128]{2,0,1:T(8,128)(2,1)S(1)}, bf16[512,4,128]{2,0,1:T(8,128)(2,1)S(1)}, u32[]{:S(2)}, u32[]{:S(2)}) %collective-permute-start.10) | collective-permute-done | bytes 524320 | tf_op jit(solution)/shard_map/ppermute | solution.py:12
  219.2 5.2 collective-permute-start.11
  224.5 6.1 %collective-permute-done.11 = bf16[512,4,128]{2,0,1:T(8,128)(2,1)} collective-permute-done((bf16[512,4,128]{2,0,1:T(8,128)(2,1)S(1)}, bf16[512,4,128]{2,0,1:T(8,128)(2,1)}, u32[]{:S(2)}, u32[]{:S(2)}) %collective-permute-start.11) | collective-permute-done | bytes 524320 | tf_op jit(solution)/shard_map/ppermute | solution.py:12
  230.6 5.3 collective-permute-start.12
  242.3 5.2 collective-permute-start.13
  253.9 5.2 collective-permute-start.14
  259.2 5.8 %fusion.77 = (f32[512]{0:T(512)S(1)}, f32[512]{0:T(512)S(1)}, f32[512,512]{1,0:T(8,128)}) fusion(f32[542,512]{1,0:T(8,128)S(1)} %maximum_convert_fusion, f32[512]{0:T(512)S(1)} %bitcast.166, f32[512]{0:T(512)S(1)} %bitcast.167, f32[512]{0:T(512)S(1)} %bitcast.138, f32[512]{0:T(512)S(1)} %bitcast.139, f32[512]{0:T(512)S(1)} %bitcast.140, ...), kind=kLoop, calls=%fused_computation.181 | loop fusion | flops 16776192 | bytes 33622016 | tf_op jit(solution)/shard_map/reduce_sum | solution.py:168
  311.2 7.2 %constant_dynamic-slice_fusion = bf16[8192,4,128]{2,0,1:T(8,128)(2,1)} fusion(bf16[16384,4,128]{2,0,1:T(8,128)(2,1)} %constant_dynamic-update-slice_fusion, s32[]{:T(128)S(6)} %select_n.25), kind=kLoop, calls=%fused_computation.180 | loop fusion | bytes 16777220 | tf_op jit(solution)/shard_map/jit(_roll_dynamic)/dynamic_slice | solution.py:15
  318.4 7.7 %copy.25 = bf16[16,512,4,128]{3,1,2,0:T(8,128)(2,1)} copy(bf16[16,512,4,128]{3,1,0,2:T(8,128)(2,1)} %bitcast.121) | data formatting | bytes 16777216
  326.1 8.0 %copy.53 = bf16[4,2,8,16,8,512]{5,4,2,1,0,3:T(8,128)(2,1)} copy(bf16[4,2,8,16,8,512]{5,4,3,2,1,0:T(8,128)(2,1)} %bitcast.124) | data formatting | bytes 16777216 | tf_op jit(solution)/shard_map/reshape | solution.py:109
  335.6 196.0 %while.15 = (s32[]{:T(128)}, f32[4,2,512]{2,1,0:T(2,128)S(1)}, f32[4,2,512]{2,1,0:T(2,128)S(1)}, f32[4,2,512,128]{3,2,1,0:T(8,128)}, s32[16]{0:T(128)S(1)}, /*in...) while((s32[]{:T(128)}, f32[4,2,512]{2,1,0:T(2,128)S(1)}, ...), condition=%wide.region_8.9_spmd.clone, body=%wide.region_3.8_spmd.clone.sunk | while | flops 833889280 | bytes 49034592 | solution.py:142
  337.1 11.0 %conditional.3 = ((f32[4,2,512]{2,1,0:T(2,128)S(1)}, f32[4,2,512]{2,1,0:T(2,128)S(1)}, f32[4,2,512,128]{3,2,1,0:T(8,128)})) conditional(s32[]{:T(128)} %convert_element_type.168, (f32[4,2,512]{2,1,0:T(2,128)S(1)}, f32[4,2,512]{2,1,0:T(2,128)S(1)}, f32[4,2,512,128]{3,2,1,0:T(8,128)}) %tuple.88, (s32[]{:T(128)}, s32[]{:T(128)}, ...), branch_computations={%region_4.4_spmd, %region_5.7_spmd} | conditional | flops 833889280 | bytes 49032288 | solution.py:140
  342.2 4.6 multiply_add_fusion
  349.3 11.0 %conditional.3 = ((f32[4,2,512]{2,1,0:T(2,128)S(1)}, f32[4,2,512]{2,1,0:T(2,128)S(1)}, f32[4,2,512,128]{3,2,1,0:T(8,128)})) conditional(s32[]{:T(128)} %convert_element_type.168, (f32[4,2,512]{2,1,0:T(2,128)S(1)}, f32[4,2,512]{2,1,0:T(2,128)S(1)}, f32[4,2,512,128]{3,2,1,0:T(8,128)}) %tuple.88, (s32[]{:T(128)}, s32[]{:T(128)}, ...), branch_computations={%region_4.4_spmd, %region_5.7_spmd} | conditional | flops 833889280 | bytes 49032288 | solution.py:140
  354.4 4.6 multiply_add_fusion
  361.6 11.0 %conditional.3 = ((f32[4,2,512]{2,1,0:T(2,128)S(1)}, f32[4,2,512]{2,1,0:T(2,128)S(1)}, f32[4,2,512,128]{3,2,1,0:T(8,128)})) conditional(s32[]{:T(128)} %convert_element_type.168, (f32[4,2,512]{2,1,0:T(2,128)S(1)}, f32[4,2,512]{2,1,0:T(2,128)S(1)}, f32[4,2,512,128]{3,2,1,0:T(8,128)}) %tuple.88, (s32[]{:T(128)}, s32[]{:T(128)}, ...), branch_computations={%region_4.4_spmd, %region_5.7_spmd} | conditional | flops 833889280 | bytes 49032288 | solution.py:140
  366.6 4.6 multiply_add_fusion
  373.8 11.0 %conditional.3 = ((f32[4,2,512]{2,1,0:T(2,128)S(1)}, f32[4,2,512]{2,1,0:T(2,128)S(1)}, f32[4,2,512,128]{3,2,1,0:T(8,128)})) conditional(s32[]{:T(128)} %convert_element_type.168, (f32[4,2,512]{2,1,0:T(2,128)S(1)}, f32[4,2,512]{2,1,0:T(2,128)S(1)}, f32[4,2,512,128]{3,2,1,0:T(8,128)}) %tuple.88, (s32[]{:T(128)}, s32[]{:T(128)}, ...), branch_computations={%region_4.4_spmd, %region_5.7_spmd} | conditional | flops 833889280 | bytes 49032288 | solution.py:140
  378.9 4.6 multiply_add_fusion
  386.0 11.0 %conditional.3 = ((f32[4,2,512]{2,1,0:T(2,128)S(1)}, f32[4,2,512]{2,1,0:T(2,128)S(1)}, f32[4,2,512,128]{3,2,1,0:T(8,128)})) conditional(s32[]{:T(128)} %convert_element_type.168, (f32[4,2,512]{2,1,0:T(2,128)S(1)}, f32[4,2,512]{2,1,0:T(2,128)S(1)}, f32[4,2,512,128]{3,2,1,0:T(8,128)}) %tuple.88, (s32[]{:T(128)}, s32[]{:T(128)}, ...), branch_computations={%region_4.4_spmd, %region_5.7_spmd} | conditional | flops 833889280 | bytes 49032288 | solution.py:140
  391.1 4.6 multiply_add_fusion
  398.3 11.0 %conditional.3 = ((f32[4,2,512]{2,1,0:T(2,128)S(1)}, f32[4,2,512]{2,1,0:T(2,128)S(1)}, f32[4,2,512,128]{3,2,1,0:T(8,128)})) conditional(s32[]{:T(128)} %convert_element_type.168, (f32[4,2,512]{2,1,0:T(2,128)S(1)}, f32[4,2,512]{2,1,0:T(2,128)S(1)}, f32[4,2,512,128]{3,2,1,0:T(8,128)}) %tuple.88, (s32[]{:T(128)}, s32[]{:T(128)}, ...), branch_computations={%region_4.4_spmd, %region_5.7_spmd} | conditional | flops 833889280 | bytes 49032288 | solution.py:140
  403.3 4.6 multiply_add_fusion
  410.5 11.0 %conditional.3 = ((f32[4,2,512]{2,1,0:T(2,128)S(1)}, f32[4,2,512]{2,1,0:T(2,128)S(1)}, f32[4,2,512,128]{3,2,1,0:T(8,128)})) conditional(s32[]{:T(128)} %convert_element_type.168, (f32[4,2,512]{2,1,0:T(2,128)S(1)}, f32[4,2,512]{2,1,0:T(2,128)S(1)}, f32[4,2,512,128]{3,2,1,0:T(8,128)}) %tuple.88, (s32[]{:T(128)}, s32[]{:T(128)}, ...), branch_computations={%region_4.4_spmd, %region_5.7_spmd} | conditional | flops 833889280 | bytes 49032288 | solution.py:140
  415.6 4.6 multiply_add_fusion
  422.7 11.0 %conditional.3 = ((f32[4,2,512]{2,1,0:T(2,128)S(1)}, f32[4,2,512]{2,1,0:T(2,128)S(1)}, f32[4,2,512,128]{3,2,1,0:T(8,128)})) conditional(s32[]{:T(128)} %convert_element_type.168, (f32[4,2,512]{2,1,0:T(2,128)S(1)}, f32[4,2,512]{2,1,0:T(2,128)S(1)}, f32[4,2,512,128]{3,2,1,0:T(8,128)}) %tuple.88, (s32[]{:T(128)}, s32[]{:T(128)}, ...), branch_computations={%region_4.4_spmd, %region_5.7_spmd} | conditional | flops 833889280 | bytes 49032288 | solution.py:140
  427.8 4.6 multiply_add_fusion
  435.0 11.0 %conditional.3 = ((f32[4,2,512]{2,1,0:T(2,128)S(1)}, f32[4,2,512]{2,1,0:T(2,128)S(1)}, f32[4,2,512,128]{3,2,1,0:T(8,128)})) conditional(s32[]{:T(128)} %convert_element_type.168, (f32[4,2,512]{2,1,0:T(2,128)S(1)}, f32[4,2,512]{2,1,0:T(2,128)S(1)}, f32[4,2,512,128]{3,2,1,0:T(8,128)}) %tuple.88, (s32[]{:T(128)}, s32[]{:T(128)}, ...), branch_computations={%region_4.4_spmd, %region_5.7_spmd} | conditional | flops 833889280 | bytes 49032288 | solution.py:140
  440.0 4.6 multiply_add_fusion
  447.2 11.0 %conditional.3 = ((f32[4,2,512]{2,1,0:T(2,128)S(1)}, f32[4,2,512]{2,1,0:T(2,128)S(1)}, f32[4,2,512,128]{3,2,1,0:T(8,128)})) conditional(s32[]{:T(128)} %convert_element_type.168, (f32[4,2,512]{2,1,0:T(2,128)S(1)}, f32[4,2,512]{2,1,0:T(2,128)S(1)}, f32[4,2,512,128]{3,2,1,0:T(8,128)}) %tuple.88, (s32[]{:T(128)}, s32[]{:T(128)}, ...), branch_computations={%region_4.4_spmd, %region_5.7_spmd} | conditional | flops 833889280 | bytes 49032288 | solution.py:140
  452.3 4.6 multiply_add_fusion
  459.4 11.0 %conditional.3 = ((f32[4,2,512]{2,1,0:T(2,128)S(1)}, f32[4,2,512]{2,1,0:T(2,128)S(1)}, f32[4,2,512,128]{3,2,1,0:T(8,128)})) conditional(s32[]{:T(128)} %convert_element_type.168, (f32[4,2,512]{2,1,0:T(2,128)S(1)}, f32[4,2,512]{2,1,0:T(2,128)S(1)}, f32[4,2,512,128]{3,2,1,0:T(8,128)}) %tuple.88, (s32[]{:T(128)}, s32[]{:T(128)}, ...), branch_computations={%region_4.4_spmd, %region_5.7_spmd} | conditional | flops 833889280 | bytes 49032288 | solution.py:140
  464.5 4.6 multiply_add_fusion
  471.7 11.0 %conditional.3 = ((f32[4,2,512]{2,1,0:T(2,128)S(1)}, f32[4,2,512]{2,1,0:T(2,128)S(1)}, f32[4,2,512,128]{3,2,1,0:T(8,128)})) conditional(s32[]{:T(128)} %convert_element_type.168, (f32[4,2,512]{2,1,0:T(2,128)S(1)}, f32[4,2,512]{2,1,0:T(2,128)S(1)}, f32[4,2,512,128]{3,2,1,0:T(8,128)}) %tuple.88, (s32[]{:T(128)}, s32[]{:T(128)}, ...), branch_computations={%region_4.4_spmd, %region_5.7_spmd} | conditional | flops 833889280 | bytes 49032288 | solution.py:140
  476.7 4.6 multiply_add_fusion
  483.9 11.0 %conditional.3 = ((f32[4,2,512]{2,1,0:T(2,128)S(1)}, f32[4,2,512]{2,1,0:T(2,128)S(1)}, f32[4,2,512,128]{3,2,1,0:T(8,128)})) conditional(s32[]{:T(128)} %convert_element_type.168, (f32[4,2,512]{2,1,0:T(2,128)S(1)}, f32[4,2,512]{2,1,0:T(2,128)S(1)}, f32[4,2,512,128]{3,2,1,0:T(8,128)}) %tuple.88, (s32[]{:T(128)}, s32[]{:T(128)}, ...), branch_computations={%region_4.4_spmd, %region_5.7_spmd} | conditional | flops 833889280 | bytes 49032288 | solution.py:140
  496.1 11.0 %conditional.3 = ((f32[4,2,512]{2,1,0:T(2,128)S(1)}, f32[4,2,512]{2,1,0:T(2,128)S(1)}, f32[4,2,512,128]{3,2,1,0:T(8,128)})) conditional(s32[]{:T(128)} %convert_element_type.168, (f32[4,2,512]{2,1,0:T(2,128)S(1)}, f32[4,2,512]{2,1,0:T(2,128)S(1)}, f32[4,2,512,128]{3,2,1,0:T(8,128)}) %tuple.88, (s32[]{:T(128)}, s32[]{:T(128)}, ...), branch_computations={%region_4.4_spmd, %region_5.7_spmd} | conditional | flops 833889280 | bytes 49032288 | solution.py:140
  508.4 11.0 %conditional.3 = ((f32[4,2,512]{2,1,0:T(2,128)S(1)}, f32[4,2,512]{2,1,0:T(2,128)S(1)}, f32[4,2,512,128]{3,2,1,0:T(8,128)})) conditional(s32[]{:T(128)} %convert_element_type.168, (f32[4,2,512]{2,1,0:T(2,128)S(1)}, f32[4,2,512]{2,1,0:T(2,128)S(1)}, f32[4,2,512,128]{3,2,1,0:T(8,128)}) %tuple.88, (s32[]{:T(128)}, s32[]{:T(128)}, ...), branch_computations={%region_4.4_spmd, %region_5.7_spmd} | conditional | flops 833889280 | bytes 49032288 | solution.py:140
  513.4 4.6 multiply_add_fusion
  520.6 11.0 %conditional.3 = ((f32[4,2,512]{2,1,0:T(2,128)S(1)}, f32[4,2,512]{2,1,0:T(2,128)S(1)}, f32[4,2,512,128]{3,2,1,0:T(8,128)})) conditional(s32[]{:T(128)} %convert_element_type.168, (f32[4,2,512]{2,1,0:T(2,128)S(1)}, f32[4,2,512]{2,1,0:T(2,128)S(1)}, f32[4,2,512,128]{3,2,1,0:T(8,128)}) %tuple.88, (s32[]{:T(128)}, s32[]{:T(128)}, ...), branch_computations={%region_4.4_spmd, %region_5.7_spmd} | conditional | flops 833889280 | bytes 49032288 | solution.py:140
  525.7 4.6 multiply_add_fusion
  540.3 7.6 %all-to-all-done = bf16[2,256,1024]{2,1,0:T(8,128)(2,1)S(1)} async-done(((bf16[2,256,1024]{2,1,0:T(8,128)(2,1)}), bf16[2,256,1024]{2,1,0:T(8,128)(2,1)S(1)}, u32[]{:S(2)}, u32[]{:S(2)}) %all-to-all-start) | async-done | bytes 1048608 | tf_op jit(solution)/shard_map/all_to_all | solution.py:180
  550.3 6.7 %fusion.23 = bf16[256,2048]{1,0:T(8,128)(2,1)} fusion(bf16[2,2,512,2048]{3,2,1,0:T(8,128)(2,1)} %bitcast.123, bf16[256,2,2,512]{0,3,2,1:T(8,128)(2,1)S(1)} %bitcast.126), kind=kOutput, calls=%fused_computation.31 | convolution fusion | flops 2148007936 | bytes 10485760 | tf_op jit(solution)/shard_map/rtcj,ctjd->rd/dot_general | solution.py:182
  (386 shorter events, 214.3 us)
Async XLA Ops:
  7.2 38.5 %copy-start = (bf16[2048,512]{1,0:T(8,128)(2,1)S(1)}, bf16[2048,512]{1,0:T(8,128)(2,1)}, u32[]{:S(2)}) copy-start(bf16[2048,512]{1,0:T(8,128)(2,1)} %param.20) | copy-start | bytes 6291460
  7.2 41.5 %copy-start.48 = (f32[2048]{0:T(1024)S(1)}, f32[2048]{0:T(1024)}, u32[]{:S(2)}) copy-start(f32[2048]{0:T(1024)} %param.19) | copy-start | bytes 24580
  7.2 36.2 %all-gather.3.cloned.1.call-start = ((), (), s32[]{:S(2)}) async-start(), calls=%async_computation.1 | async-start | bytes 3145728 | tf_op jit(solution)/shard_map/all_gather | solution.py:81
  7.9 318.2 %all-gather.5.cloned.1.call-start = ((), (), s32[]{:S(2)}) async-start(), calls=%async_computation.2 | async-start | bytes 8912896 | tf_op jit(solution)/shard_map/all_gather | solution.py:104
  43.4 5.3 copy-start.5
  43.4 5.3 copy-start.47
  45.7 6.8 %copy-start.43 = (f32[512]{0:T(512)}, f32[512]{0:T(512)S(1)}, u32[]{:S(2)}) copy-start(f32[512]{0:T(512)S(1)} %add_rsqrt_fusion.4) | copy-start | bytes 6148
  50.2 174.2 %copy-start.29 = (f32[31,512]{1,0:T(8,128)S(1)}, f32[31,512]{1,0:T(8,128)}, u32[]{:S(2)}) copy-start(f32[31,512]{1,0:T(8,128)} %param.28) | copy-start | bytes 190468
  52.5 194.9 %copy-start.6 = (bf16[512,2048]{1,0:T(8,128)(2,1)S(1)}, bf16[512,2048]{1,0:T(8,128)(2,1)}, u32[]{:S(2)}) copy-start(bf16[512,2048]{1,0:T(8,128)(2,1)} %all-gather.3.cloned.1.call-done) | copy-start | bytes 6291460
  56.6 10.0 %collective-permute-start = (bf16[512,4,128]{2,0,1:T(8,128)(2,1)S(1)}, bf16[512,4,128]{2,0,1:T(8,128)(2,1)S(1)}, u32[]{:S(2)}, u32[]{:S(2)}) collective-permute-start(bf16[512,4,128]{2,0,1:T(8,128)(2,1)S(1)} %copy.21), channel_id=1, source_target_pairs={{0,2},{2,4},{4,6},{6,8},{8,10},{10,12},{12,14},{14,16},{16,18},{18... | collective-permute-start | bytes 1572872 | tf_op jit(solution)/shard_map/ppermute | solution.py:12
  66.6 22.1 %collective-permute-start.1 = (bf16[512,4,128]{2,0,1:T(8,128)(2,1)S(1)}, bf16[512,4,128]{2,0,1:T(8,128)(2,1)S(1)}, u32[]{:S(2)}, u32[]{:S(2)}) collective-permute-start(bf16[512,4,128]{2,0,1:T(8,128)(2,1)S(1)} %collective-permute-done), channel_id=1, source_target_pairs={{0,2},{2,4},{4,6},{6,8},{8,10},{10,12},{12,14},{14,16},{16,18},{18... | collective-permute-start | bytes 1572872 | tf_op jit(solution)/shard_map/ppermute | solution.py:12
  89.5 21.8 %collective-permute-start.2 = (bf16[512,4,128]{2,0,1:T(8,128)(2,1)S(1)}, bf16[512,4,128]{2,0,1:T(8,128)(2,1)S(1)}, u32[]{:S(2)}, u32[]{:S(2)}) collective-permute-start(bf16[512,4,128]{2,0,1:T(8,128)(2,1)S(1)} %collective-permute-done.1), channel_id=1, source_target_pairs={{0,2},{2,4},{4,6},{6,8},{8,10},{10,12},{12,14},{14,16},{16,18},{18... | collective-permute-start | bytes 1572872 | tf_op jit(solution)/shard_map/ppermute | solution.py:12
  112.0 20.9 %collective-permute-start.3 = (bf16[512,4,128]{2,0,1:T(8,128)(2,1)S(1)}, bf16[512,4,128]{2,0,1:T(8,128)(2,1)S(1)}, u32[]{:S(2)}, u32[]{:S(2)}) collective-permute-start(bf16[512,4,128]{2,0,1:T(8,128)(2,1)S(1)} %collective-permute-done.2), channel_id=1, source_target_pairs={{0,2},{2,4},{4,6},{6,8},{8,10},{10,12},{12,14},{14,16},{16,18},{18... | collective-permute-start | bytes 1572872 | tf_op jit(solution)/shard_map/ppermute | solution.py:12
  133.8 12.1 %collective-permute-start.4 = (bf16[512,4,128]{2,0,1:T(8,128)(2,1)S(1)}, bf16[512,4,128]{2,0,1:T(8,128)(2,1)S(1)}, u32[]{:S(2)}, u32[]{:S(2)}) collective-permute-start(bf16[512,4,128]{2,0,1:T(8,128)(2,1)S(1)} %collective-permute-done.3), channel_id=1, source_target_pairs={{0,2},{2,4},{4,6},{6,8},{8,10},{10,12},{12,14},{14,16},{16,18},{18... | collective-permute-start | bytes 1572872 | tf_op jit(solution)/shard_map/ppermute | solution.py:12
  146.6 11.3 %collective-permute-start.5 = (bf16[512,4,128]{2,0,1:T(8,128)(2,1)S(1)}, bf16[512,4,128]{2,0,1:T(8,128)(2,1)S(1)}, u32[]{:S(2)}, u32[]{:S(2)}) collective-permute-start(bf16[512,4,128]{2,0,1:T(8,128)(2,1)S(1)} %collective-permute-done.4), channel_id=1, source_target_pairs={{0,2},{2,4},{4,6},{6,8},{8,10},{10,12},{12,14},{14,16},{16,18},{18... | collective-permute-start | bytes 1572872 | tf_op jit(solution)/shard_map/ppermute | solution.py:12
  158.8 11.3 %collective-permute-start.6 = (bf16[512,4,128]{2,0,1:T(8,128)(2,1)S(1)}, bf16[512,4,128]{2,0,1:T(8,128)(2,1)S(1)}, u32[]{:S(2)}, u32[]{:S(2)}) collective-permute-start(bf16[512,4,128]{2,0,1:T(8,128)(2,1)S(1)} %collective-permute-done.5), channel_id=1, source_target_pairs={{0,2},{2,4},{4,6},{6,8},{8,10},{10,12},{12,14},{14,16},{16,18},{18... | collective-permute-start | bytes 1572872 | tf_op jit(solution)/shard_map/ppermute | solution.py:12
  170.9 11.3 %collective-permute-start.7 = (bf16[512,4,128]{2,0,1:T(8,128)(2,1)S(1)}, bf16[512,4,128]{2,0,1:T(8,128)(2,1)S(1)}, u32[]{:S(2)}, u32[]{:S(2)}) collective-permute-start(bf16[512,4,128]{2,0,1:T(8,128)(2,1)S(1)} %collective-permute-done.6), channel_id=1, source_target_pairs={{0,2},{2,4},{4,6},{6,8},{8,10},{10,12},{12,14},{14,16},{16,18},{18... | collective-permute-start | bytes 1572872 | tf_op jit(solution)/shard_map/ppermute | solution.py:12
  183.0 11.3 %collective-permute-start.8 = (bf16[512,4,128]{2,0,1:T(8,128)(2,1)S(1)}, bf16[512,4,128]{2,0,1:T(8,128)(2,1)S(1)}, u32[]{:S(2)}, u32[]{:S(2)}) collective-permute-start(bf16[512,4,128]{2,0,1:T(8,128)(2,1)S(1)} %collective-permute-done.7), channel_id=1, source_target_pairs={{0,2},{2,4},{4,6},{6,8},{8,10},{10,12},{12,14},{14,16},{16,18},{18... | collective-permute-start | bytes 1572872 | tf_op jit(solution)/shard_map/ppermute | solution.py:12
  195.0 11.3 %collective-permute-start.9 = (bf16[512,4,128]{2,0,1:T(8,128)(2,1)S(1)}, bf16[512,4,128]{2,0,1:T(8,128)(2,1)S(1)}, u32[]{:S(2)}, u32[]{:S(2)}) collective-permute-start(bf16[512,4,128]{2,0,1:T(8,128)(2,1)S(1)} %collective-permute-done.8), channel_id=1, source_target_pairs={{0,2},{2,4},{4,6},{6,8},{8,10},{10,12},{12,14},{14,16},{16,18},{18... | collective-permute-start | bytes 1572872 | tf_op jit(solution)/shard_map/ppermute | solution.py:12
  207.1 11.3 %collective-permute-start.10 = (bf16[512,4,128]{2,0,1:T(8,128)(2,1)S(1)}, bf16[512,4,128]{2,0,1:T(8,128)(2,1)S(1)}, u32[]{:S(2)}, u32[]{:S(2)}) collective-permute-start(bf16[512,4,128]{2,0,1:T(8,128)(2,1)S(1)} %collective-permute-done.9), channel_id=1, source_target_pairs={{0,2},{2,4},{4,6},{6,8},{8,10},{10,12},{12,14},{14,16},{16,18},{18... | collective-permute-start | bytes 1572872 | tf_op jit(solution)/shard_map/ppermute | solution.py:12
  219.2 11.3 %collective-permute-start.11 = (bf16[512,4,128]{2,0,1:T(8,128)(2,1)S(1)}, bf16[512,4,128]{2,0,1:T(8,128)(2,1)}, u32[]{:S(2)}, u32[]{:S(2)}) collective-permute-start(bf16[512,4,128]{2,0,1:T(8,128)(2,1)S(1)} %collective-permute-done.10), channel_id=1, source_target_pairs={{0,2},{2,4},{4,6},{6,8},{8,10},{10,12},{12,14},{14,16},{16,18},{18... | collective-permute-start | bytes 1572872 | tf_op jit(solution)/shard_map/ppermute | solution.py:12
  230.6 11.7 %collective-permute-start.12 = (bf16[512,4,128]{2,0,1:T(8,128)(2,1)}, bf16[512,4,128]{2,0,1:T(8,128)(2,1)}, u32[]{:S(2)}, u32[]{:S(2)}) collective-permute-start(bf16[512,4,128]{2,0,1:T(8,128)(2,1)} %collective-permute-done.11), channel_id=1, source_target_pairs={{0,2},{2,4},{4,6},{6,8},{8,10},{10,12},{12,14},{14,16},{16,18},{18... | collective-permute-start | bytes 1572872 | tf_op jit(solution)/shard_map/ppermute | solution.py:12
  240.0 11.9 %copy-start.28 = (bf16[512,4,2,32]{0,3,2,1:T(8,128)(2,1)S(1)}, bf16[512,4,2,32]{0,3,2,1:T(8,128)(2,1)}, u32[]{:S(2)}) copy-start(bf16[512,4,2,32]{0,3,2,1:T(8,128)(2,1)} %get-tuple-element.215) | copy-start | bytes 786436
  240.0 19.1 %copy-start.30 = (f32[1,512]{1,0:T(1,128)S(1)}, f32[1,512]{1,0:T(1,128)}, u32[]{:S(2)}) copy-start(f32[1,512]{1,0:T(1,128)} %get-tuple-element.240) | copy-start | bytes 6148
  240.0 19.1 %copy-start.31 = (f32[1,512]{1,0:T(1,128)S(1)}, f32[1,512]{1,0:T(1,128)}, u32[]{:S(2)}) copy-start(f32[1,512]{1,0:T(1,128)} %get-tuple-element.241) | copy-start | bytes 6148
  240.0 19.0 %copy-start.32 = (f32[1,512]{1,0:T(1,128)S(1)}, f32[1,512]{1,0:T(1,128)}, u32[]{:S(2)}) copy-start(f32[1,512]{1,0:T(1,128)} %get-tuple-element.242) | copy-start | bytes 6148
  240.0 19.0 %copy-start.33 = (f32[1,512]{1,0:T(1,128)S(1)}, f32[1,512]{1,0:T(1,128)}, u32[]{:S(2)}) copy-start(f32[1,512]{1,0:T(1,128)} %get-tuple-element.243) | copy-start | bytes 6148
  240.1 19.0 %copy-start.34 = (f32[1,512]{1,0:T(1,128)S(1)}, f32[1,512]{1,0:T(1,128)}, u32[]{:S(2)}) copy-start(f32[1,512]{1,0:T(1,128)} %get-tuple-element.244) | copy-start | bytes 6148
  240.1 19.0 %copy-start.35 = (f32[1,512]{1,0:T(1,128)S(1)}, f32[1,512]{1,0:T(1,128)}, u32[]{:S(2)}) copy-start(f32[1,512]{1,0:T(1,128)} %get-tuple-element.245) | copy-start | bytes 6148
  240.1 19.0 %copy-start.36 = (f32[1,512]{1,0:T(1,128)S(1)}, f32[1,512]{1,0:T(1,128)}, u32[]{:S(2)}) copy-start(f32[1,512]{1,0:T(1,128)} %get-tuple-element.246) | copy-start | bytes 6148
  240.1 19.0 %copy-start.37 = (f32[1,512]{1,0:T(1,128)S(1)}, f32[1,512]{1,0:T(1,128)}, u32[]{:S(2)}) copy-start(f32[1,512]{1,0:T(1,128)} %get-tuple-element.247) | copy-start | bytes 6148
  240.1 19.0 %copy-start.38 = (f32[1,512]{1,0:T(1,128)S(1)}, f32[1,512]{1,0:T(1,128)}, u32[]{:S(2)}) copy-start(f32[1,512]{1,0:T(1,128)} %get-tuple-element.248) | copy-start | bytes 6148
  240.1 19.0 %copy-start.39 = (f32[1,512]{1,0:T(1,128)S(1)}, f32[1,512]{1,0:T(1,128)}, u32[]{:S(2)}) copy-start(f32[1,512]{1,0:T(1,128)} %get-tuple-element.249) | copy-start | bytes 6148
  240.1 19.0 %copy-start.40 = (f32[1,512]{1,0:T(1,128)S(1)}, f32[1,512]{1,0:T(1,128)}, u32[]{:S(2)}) copy-start(f32[1,512]{1,0:T(1,128)} %get-tuple-element.250) | copy-start | bytes 6148
  242.3 11.6 %collective-permute-start.13 = (bf16[512,4,128]{2,0,1:T(8,128)(2,1)}, bf16[512,4,128]{2,0,1:T(8,128)(2,1)}, u32[]{:S(2)}, u32[]{:S(2)}) collective-permute-start(bf16[512,4,128]{2,0,1:T(8,128)(2,1)} %collective-permute-done.12), channel_id=1, source_target_pairs={{0,2},{2,4},{4,6},{6,8},{8,10},{10,12},{12,14},{14,16},{16,18},{18... | collective-permute-start | bytes 1572872 | tf_op jit(solution)/shard_map/ppermute | solution.py:12
  250.6 3.1 collective-permute-start.15
  253.9 17.6 %collective-permute-start.14 = (bf16[512,4,128]{2,0,1:T(8,128)(2,1)}, bf16[512,4,128]{2,0,1:T(8,128)(2,1)}, u32[]{:S(2)}, u32[]{:S(2)}) collective-permute-start(bf16[512,4,128]{2,0,1:T(8,128)(2,1)} %collective-permute-done.13), channel_id=1, source_target_pairs={{0,2},{2,4},{4,6},{6,8},{8,10},{10,12},{12,14},{14,16},{16,18},{18... | collective-permute-start | bytes 1572872 | tf_op jit(solution)/shard_map/ppermute | solution.py:12
  259.2 9.7 %copy-start.41 = (f32[512]{0:T(512)S(1)}, f32[512]{0:T(512)}, u32[]{:S(2)}) copy-start(f32[512]{0:T(512)} %param.30) | copy-start | bytes 6148
  259.2 9.7 %copy-start.42 = (f32[512]{0:T(512)S(1)}, f32[512]{0:T(512)}, u32[]{:S(2)}) copy-start(f32[512]{0:T(512)} %param.29) | copy-start | bytes 6148
  264.9 23.7 %copy-start.12 = (bf16[512,4,128]{2,0,1:T(8,128)(2,1)S(1)}, bf16[512,4,128]{2,0,1:T(8,128)(2,1)}, u32[]{:S(2)}) copy-start(bf16[512,4,128]{2,0,1:T(8,128)(2,1)} %copy-done.11) | copy-start | bytes 1572868
  264.9 24.6 %copy-start.10 = (bf16[512,4,128]{2,0,1:T(8,128)(2,1)S(1)}, bf16[512,4,128]{2,0,1:T(8,128)(2,1)}, u32[]{:S(2)}) copy-start(bf16[512,4,128]{2,0,1:T(8,128)(2,1)} %copy-done.9) | copy-start | bytes 1572868
  265.0 25.4 %copy-start.8 = (bf16[512,4,128]{2,0,1:T(8,128)(2,1)S(1)}, bf16[512,4,128]{2,0,1:T(8,128)(2,1)}, u32[]{:S(2)}) copy-start(bf16[512,4,128]{2,0,1:T(8,128)(2,1)} %copy-done.7) | copy-start | bytes 1572868
  268.9 16.3 %copy-start.20 = (bf16[512,4,128]{2,0,1:T(8,128)(2,1)S(1)}, bf16[512,4,128]{2,0,1:T(8,128)(2,1)}, u32[]{:S(2)}) copy-start(bf16[512,4,128]{2,0,1:T(8,128)(2,1)} %copy-done.19) | copy-start | bytes 1572868
  268.9 17.1 %copy-start.18 = (bf16[512,4,128]{2,0,1:T(8,128)(2,1)S(1)}, bf16[512,4,128]{2,0,1:T(8,128)(2,1)}, u32[]{:S(2)}) copy-start(bf16[512,4,128]{2,0,1:T(8,128)(2,1)} %copy-done.17) | copy-start | bytes 1572868
  268.9 18.0 %copy-start.16 = (bf16[512,4,128]{2,0,1:T(8,128)(2,1)S(1)}, bf16[512,4,128]{2,0,1:T(8,128)(2,1)}, u32[]{:S(2)}) copy-start(bf16[512,4,128]{2,0,1:T(8,128)(2,1)} %copy-done.15) | copy-start | bytes 1572868
  268.9 18.9 %copy-start.14 = (bf16[512,4,128]{2,0,1:T(8,128)(2,1)S(1)}, bf16[512,4,128]{2,0,1:T(8,128)(2,1)}, u32[]{:S(2)}) copy-start(bf16[512,4,128]{2,0,1:T(8,128)(2,1)} %copy-done.13) | copy-start | bytes 1572868
  279.2 21.5 %copy-start.27 = (bf16[512,4,128]{2,0,1:T(8,128)(2,1)S(1)}, bf16[512,4,128]{2,0,1:T(8,128)(2,1)}, u32[]{:S(2)}) copy-start(bf16[512,4,128]{2,0,1:T(8,128)(2,1)} %copy-done.26) | copy-start | bytes 1572868
  281.2 20.4 %copy-start.24 = (bf16[512,4,128]{2,0,1:T(8,128)(2,1)S(1)}, bf16[512,4,128]{2,0,1:T(8,128)(2,1)}, u32[]{:S(2)}) copy-start(bf16[512,4,128]{2,0,1:T(8,128)(2,1)} %copy-done.23) | copy-start | bytes 1572868
  283.1 19.3 %copy-start.22 = (bf16[512,4,128]{2,0,1:T(8,128)(2,1)S(1)}, bf16[512,4,128]{2,0,1:T(8,128)(2,1)}, u32[]{:S(2)}) copy-start(bf16[512,4,128]{2,0,1:T(8,128)(2,1)} %copy-done.21) | copy-start | bytes 1572868
  335.6 196.1 %copy-start.46 = (f32[4]{0:T(128)S(1)}, f32[4]{0:T(128)}, u32[]{:S(2)}) copy-start(f32[4]{0:T(128)} %param.26) | copy-start | bytes 52
  335.6 198.3 %copy-start.45 = (f32[128]{0:T(128)S(1)}, f32[128]{0:T(128)}, u32[]{:S(2)}) copy-start(f32[128]{0:T(128)} %param.27) | copy-start | bytes 1540
  335.6 199.3 %copy-start.25 = (bf16[512,512]{1,0:T(8,128)(2,1)S(1)}, bf16[512,512]{1,0:T(8,128)(2,1)}, u32[]{:S(2)}) copy-start(bf16[512,512]{1,0:T(8,128)(2,1)} %multiply_convert_fusion) | copy-start | bytes 1572868
  337.4 4.8 copy-start.2
  349.6 4.8 copy-start.2
  374.1 4.8 copy-start.2
  386.3 4.8 copy-start.2
  398.5 4.8 copy-start.2
  423.0 4.8 copy-start.2
  435.2 4.8 copy-start.2
  447.5 4.8 copy-start.2
  484.2 4.8 copy-start.2
  496.4 4.8 copy-start.2
  534.9 22.1 %copy-start.1 = (bf16[2048,512]{1,0:T(8,128)(2,1)S(1)}, bf16[2048,512]{1,0:T(8,128)(2,1)}, u32[]{:S(2)}) copy-start(bf16[2048,512]{1,0:T(8,128)(2,1)} %param.20) | copy-start | bytes 6291460
  536.0 11.8 %all-to-all-start = ((bf16[2,256,1024]{2,1,0:T(8,128)(2,1)}), bf16[2,256,1024]{2,1,0:T(8,128)(2,1)S(1)}, u32[]{:S(2)}, u32[]{:S(2)}) async-start(bf16[2,256,1024]{2,1,0:T(8,128)(2,1)} %pad_maximum_fusion), calls=%async_computation | async-start | bytes 2097152 | tf_op jit(solution)/shard_map/all_to_all | solution.py:180
  (34 other events, 63.8 us)
Sparse Core Ops, SparseCore 0:
  9.5 33.8 all-gather.2
  52.7 91.2 all-gather.4
